TPU v7x, 32 devices: a whole 2x2x4 slice. The times are simulated.
32 devices in a mesh: rep: 2 (over y), fs: 4 (over z), tp: 4 (over x, core).
Axes of the slice: x: 2, y: 2, z: 4, core: 2. Of those that a mesh axis runs over, the one named last changes fastest.
Arguments:
- gate_pre: bfloat16 [8192, 3072], P(('rep', 'fs'), 'tp'), may hold values from -6 to 6
- up_pre: bfloat16 [8192, 3072], P(('rep', 'fs'), 'tp'), may hold values from -6 to 6
- out_grad: bfloat16 [8192, 2048], P(('rep', 'fs')), may hold values from -8 to 8
- w_down: bfloat16 [3072, 2048], P('tp', 'fs'), may hold values from -0.109375 to 0.109375
Outputs:
- d_gate: bfloat16 [8192, 3072], P(('rep', 'fs'), 'tp')
- d_up: bfloat16 [8192, 3072], P(('rep', 'fs'), 'tp')
- grad_down: float32 [3072, 2048], P('tp', 'fs')
- row_energy: float32 [3072], P('tp')
All inputs are finite; a program needn't handle non-finite values.
Results may differ from a plain program's by a relative error of at most 0.0034.
Values may be sent and summed in bfloat16 or wider, within the bound.
A program may use at most 64 MiB of HBM per device.

v0:
```python
import jax
import jax.numpy as jnp
from jax import lax
from jax.sharding import PartitionSpec as P

D = 2048


def local(gate_pre, up_pre, out_grad, w_down):
    gate_f = gate_pre.astype(jnp.float32)
    up_f = up_pre.astype(jnp.float32)
    sig = jax.nn.sigmoid(gate_f)
    act = gate_f * sig
    hidden = (act * up_f).astype(jnp.bfloat16)
    tokens_all = out_grad.shape[0] * lax.axis_size("rep") * lax.axis_size("fs")
    factor = float(tokens_all) ** (-0.5)
    weight_whole = lax.all_gather(w_down, "fs", axis=1, tiled=True)
    dhid = lax.dot_general(
        out_grad, weight_whole, (((1,), (1,)), ((), ())), preferred_element_type=jnp.float32
    )
    d_up = (dhid * act).astype(jnp.bfloat16)
    d_gate = (dhid * up_f * sig * (1.0 + gate_f * (1.0 - sig))).astype(jnp.bfloat16)
    d_gate, d_up = (d_gate, d_up)
    shard = lax.psum_scatter(
        lax.dot_general(
            out_grad, hidden, (((0,), (0,)), ((), ())), preferred_element_type=jnp.float32
        ),
        "fs",
        scatter_dimension=0,
        tiled=True,
    )
    shard = lax.psum(shard, "rep")
    grad_down = shard.T * factor
    energy = lax.psum(jnp.sum(grad_down * grad_down, axis=1), "fs") / D
    return (d_gate, d_up, grad_down, energy)


def solution(mesh):
    placed = (P(("rep", "fs"), "tp"), P(("rep", "fs"), "tp"), P(("rep", "fs"), None), P("tp", "fs"))
    return jax.shard_map(
        local,
        mesh=mesh,
        in_specs=placed,
        out_specs=(P(("rep", "fs"), "tp"), P(("rep", "fs"), "tp"), P("tp", "fs"), P("tp")),
        check_vma=False,
    )
```

profile of v0, /device:TPU:0, one launch (start us, length us, event | category | flops | bytes accessed | tf_op | source)
XLA Modules:
  0.0 269.9 jit_solution(15199787096322260005)
XLA Ops:
  7.2 0.0 reduce-scatter.2.cloned.1.call-start
  7.2 9.4 %convolution_bitcast_fusion = f32[2048,768]{0,1:T(8,128)} fusion(bf16[1024,2048]{1,0:T(8,128)(2,1)} %param.6, bf16[1024,768]{1,0:T(8,128)(2,1)} %param.5, bf16[1024,768]{1,0:T(8,128)(2,1)} %param.4), kind=kOutput, calls=%fused_computation.5 | convolution fusion | flops 3227516928 | bytes 13631488 | tf_op jit(solution)/shard_map/dot_general | solution.py:25
  16.6 0.0 copy-start
  16.7 0.0 copy-start.1
  16.7 0.0 reduce-scatter.2.cloned.1.call-update
  16.7 0.0 all-gather.2.cloned.1.call-start
  16.7 0.7 all-gather.2.cloned.1.call-update
  17.4 0.0 all-reduce.2.cloned.1.call-start
  17.5 112.9 %reduce-scatter.2.cloned.1.call-done = f32[512,768]{0,1:T(8,128)} async-done(((f32[2048,768]{0,1:T(8,128)}), f32[512,768]{0,1:T(8,128)}) %reduce-scatter.2.cloned.1.call-update) | async-done | bytes 1572880 | tf_op jit(solution)/shard_map/reduce_scatter | solution.py:24
  130.4 0.0 all-reduce.2.cloned.1.call-update
  130.4 65.5 %all-gather.2.cloned.1.call-done = bf16[768,2048]{1,0:T(8,128)(2,1)} async-done(((bf16[768,512]{1,0:T(8,128)(2,1)}), bf16[768,2048]{1,0:T(8,128)(2,1)}) %all-gather.2.cloned.1.call-update) | async-done | bytes 3145744 | tf_op jit(solution)/shard_map/all_gather | solution.py:17
  195.9 0.0 copy-done
  195.9 0.0 copy-done.1
  195.9 9.2 %multiply_convert_fusion = (bf16[1024,768]{1,0:T(8,128)(2,1)}, bf16[1024,768]{1,0:T(8,128)(2,1)}) fusion(bf16[1024,768]{1,0:T(8,128)(2,1)S(1)} %copy-done, bf16[1024,768]{1,0:T(8,128)(2,1)S(1)} %copy-done.1, bf16[1024,2048]{1,0:T(8,128)(2,1)} %param.6, bf16[768,2048]{1,0:T(8,128)(2,1)} %all-gather.2.cloned.1.call-done), kind=kOutput, calls=%fused_computation.14 | convolution fusion | flops 3233021952 | bytes 13631488 | tf_op jit(solution)/shard_map/dot_general | solution.py:18
  205.0 43.4 %all-reduce.2.cloned.1.call-done = f32[512,768]{0,1:T(8,128)} async-done(((f32[512,768]{0,1:T(8,128)}), f32[512,768]{0,1:T(8,128)}) %all-reduce.2.cloned.1.call-update) | async-done | bytes 1572880 | tf_op jit(solution)/shard_map/psum | solution.py:32
  248.4 2.7 multiply_reduce_fusion
  251.1 11.7 %psum.15 = f32[768]{0:T(1024)S(1)} all-reduce(f32[768]{0:T(1024)S(1)} %get-tuple-element.4), channel_id=1, replica_groups=mesh['rep'=2,'fs'=4,'tp'=4] {'fs'}, use_global_device_ids=true, to_apply=%region_3.0 | all-reduce | flops 768 | bytes 6144 | tf_op jit(solution)/shard_map/psum | solution.py:34
  262.8 0.6 broadcast_multiply_fusion
Async XLA Ops:
  7.2 123.2 %reduce-scatter.2.cloned.1.call-start = ((), (), s32[]{:S(2)}) async-start(), calls=%async_computation.2 | async-start | bytes 7864320 | tf_op jit(solution)/shard_map/reduce_scatter | solution.py:24
  16.6 179.2 %copy-start = (bf16[1024,768]{1,0:T(8,128)(2,1)S(1)}, bf16[1024,768]{1,0:T(8,128)(2,1)}, u32[]{:S(2)}) copy-start(bf16[1024,768]{1,0:T(8,128)(2,1)} %param.4) | copy-start | bytes 4718596
  16.7 179.2 %copy-start.1 = (bf16[1024,768]{1,0:T(8,128)(2,1)S(1)}, bf16[1024,768]{1,0:T(8,128)(2,1)}, u32[]{:S(2)}) copy-start(bf16[1024,768]{1,0:T(8,128)(2,1)} %param.5) | copy-start | bytes 4718596
  16.7 179.2 %all-gather.2.cloned.1.call-start = ((), (), s32[]{:S(2)}) async-start(), calls=%async_computation.1 | async-start | bytes 3932160 | tf_op jit(solution)/shard_map/all_gather | solution.py:17
  17.4 231.0 %all-reduce.2.cloned.1.call-start = ((), (), s32[]{:S(2)}) async-start(), calls=%async_computation.3 | async-start | bytes 3145728 | tf_op jit(solution)/shard_map/psum | solution.py:32
Sparse Core Ops, SparseCore 0:
  16.8 113.5 reduce-scatter.1
  131.9 63.9 all-gather.1
  198.2 50.1 all-reduce.1
where the time goes:
time: 270 us
  waiting for transfers between devices  222 us (82%)
  matrix products  18.6 us (7%)
  between operations  13.7 us (5%)
  blocking collectives  11.7 us (4%)
  other arithmetic  3.29 us (1%)
    reduce_scatter x1, waiting for transfers between devices, local(): lax.psum_scatter(lax.dot_general(out_grad, hidden, (((0,), (0,)), ((), ()...  113 us
    all_gather x1, waiting for transfers between devices, local(): weight_whole = lax.all_gather(w_down, 'fs', axis=1, tiled=True)  65.5 us
    psum x1, waiting for transfers between devices, local(): shard = lax.psum(shard, 'rep')  43.4 us
    psum x1, blocking collectives, local(): energy = lax.psum(jnp.sum(grad_down * grad_down, axis=1), 'fs') / D  11.7 us
    dot_general x1, matrix products, local(): lax.dot_general(out_grad, hidden, (((0,), (0,)), ((), ())), preferred_ele...  9.44 us
    dot_general x1, matrix products, local(): lax.dot_general(out_grad, weight_whole, (((1,), (1,)), ((), ())), preferr...  9.15 us
  transfers between devices with their start and end apart: 3, of which 3 were waited for; matrix products, arithmetic and copies ran while one was open for 3% of the time, Pallas kernels for 0%

commit v1 on v0

--- a/solution.py
+++ b/solution.py
@@ -4,6 +4,16 @@
 from jax.sharding import PartitionSpec as P
 
 D = 2048
+
+
+def pass_along(x, name, along):
+    devices = lax.axis_size(name)
+    moving, shards = (x, [x])
+    for _ in range(devices - 1):
+        moving = lax.ppermute(moving, name, [(i, (i + 1) % devices) for i in range(devices)])
+        shards.insert(0, moving)
+    line = jnp.concatenate(shards, axis=along)
+    return jnp.roll(line, (lax.axis_index(name) + 1) * x.shape[along], axis=along)
 
 
 def local(gate_pre, up_pre, out_grad, w_down):
@@ -14,7 +24,7 @@
     hidden = (act * up_f).astype(jnp.bfloat16)
     tokens_all = out_grad.shape[0] * lax.axis_size("rep") * lax.axis_size("fs")
     factor = float(tokens_all) ** (-0.5)
-    weight_whole = lax.all_gather(w_down, "fs", axis=1, tiled=True)
+    weight_whole = pass_along(w_down, "fs", 1)
     dhid = lax.dot_general(
         out_grad, weight_whole, (((1,), (1,)), ((), ())), preferred_element_type=jnp.float32
     )

time: 270 us -> 255 us (0.944)
  waiting for transfers between devices: 222 us -> 164 us
  starting transfers between devices: 0.12 us -> 29.3 us
  local copies, waits for them, and re-layouts: 0.01 us -> 15.6 us
    ppermute x0 -> x3, waiting for transfers between devices: none -> 106 us  [pass_along(): lax.ppermute(moving, name, [(i, (i + 1) % devices) for i in range(devices)])]
    reduce_scatter x1, waiting for transfers between devices: 113 us -> 18.9 us  [local(): lax.psum_scatter(lax.dot_general(out_grad, hidden, (((0,), (0,)), ((), ()...]
    all_gather x1 -> x0, waiting for transfers between devices: 65.5 us -> none  [local(): weight_whole = lax.all_gather(w_down, 'fs', axis=1, tiled=True)]
    ppermute x0 -> x3, starting transfers between devices: none -> 29.2 us  [pass_along(): lax.ppermute(moving, name, [(i, (i + 1) % devices) for i in range(devices)])]
    unnamed x4 -> x21, local copies, waits for them, and re-layouts: 0.01 us -> 14.6 us
    psum x1, waiting for transfers between devices: 43.4 us -> 39.4 us  [local(): shard = lax.psum(shard, 'rep')]
  transfers between devices with their start and end apart: 3 -> 5, of which waited for: 3 -> 5; matrix products, arithmetic and copies ran while one was open for 3% -> 7% of each run, Pallas kernels for 0% -> 0%
where the time goes in v1:
time: 255 us
  waiting for transfers between devices  164 us (64%)
  starting transfers between devices  29.3 us (11%)
  matrix products  16.6 us (7%)
  local copies, waits for them, and re-layouts  15.6 us (6%)
  between operations  14.1 us (6%)
  blocking collectives  11.7 us (5%)
  other arithmetic  3.29 us (1%)
    ppermute x3, waiting for transfers between devices, pass_along(): lax.ppermute(moving, name, [(i, (i + 1) % devices) for i in range(devices)])  106 us
    psum x1, waiting for transfers between devices, local(): shard = lax.psum(shard, 'rep')  39.4 us
    ppermute x3, starting transfers between devices, pass_along(): lax.ppermute(moving, name, [(i, (i + 1) % devices) for i in range(devices)])  29.2 us
    reduce_scatter x1, waiting for transfers between devices, local(): lax.psum_scatter(lax.dot_general(out_grad, hidden, (((0,), (0,)), ((), ()...  18.9 us
    unnamed x21, local copies, waits for them, and re-layouts  14.6 us
    psum x1, blocking collectives, local(): energy = lax.psum(jnp.sum(grad_down * grad_down, axis=1), 'fs') / D  11.7 us
    dot_general x1, matrix products, local(): lax.dot_general(out_grad, hidden, (((0,), (0,)), ((), ())), preferred_ele...  8.95 us
    dot_general x1, matrix products, local(): lax.dot_general(out_grad, weight_whole, (((1,), (1,)), ((), ())), preferr...  7.65 us
  transfers between devices with their start and end apart: 5, of which 5 were waited for; matrix products, arithmetic and copies ran while one was open for 7% of the time, Pallas kernels for 0%

profile of v1, /device:TPU:0, one launch (start us, length us, event | category | flops | bytes accessed | tf_op | source)
XLA Modules:
  0.0 255.0 jit_solution(8566976605577621541)
XLA Ops:
  7.2 0.0 copy-start.1
  7.2 0.0 reduce-scatter.2.cloned.1.call-start
  7.2 1.8 copy.8
  9.1 0.0 copy-done.1
  9.1 0.0 copy-start.2
  9.1 1.6 copy.9
  10.7 9.0 %convolution_bitcast_fusion = f32[2048,768]{0,1:T(8,128)} fusion(bf16[1024,2048]{1,0:T(8,128)(2,1)} %param.6, bf16[1024,768]{0,1:T(8,128)(2,1)S(1)} %copy.8, bf16[1024,768]{0,1:T(8,128)(2,1)} %copy.9), kind=kOutput, calls=%fused_computation.5 | convolution fusion | flops 3227516928 | bytes 13631488 | tf_op jit(solution)/shard_map/dot_general | solution.py:35
  19.7 0.0 copy-done.2
  19.7 0.0 copy-start
  19.7 0.0 reduce-scatter.2.cloned.1.call-update
  19.7 0.0 all-reduce.2.cloned.1.call-start
  19.8 1.1 copy-done
  20.8 3.1 %collective-permute-start = (bf16[768,512]{1,0:T(8,128)(2,1)S(1)}, bf16[768,512]{1,0:T(8,128)(2,1)S(1)}, u32[]{:S(2)}, u32[]{:S(2)}) collective-permute-start(bf16[768,512]{1,0:T(8,128)(2,1)S(1)} %copy-done), channel_id=1, source_target_pairs={{0,4},{4,8},{8,12},{12,0},{1,5},{5,9},{9,13},{13,1},{2,6},{6,10},{... | collective-permute-start | bytes 2359304 | tf_op jit(solution)/shard_map/ppermute | solution.py:13
  23.9 31.5 %collective-permute-done = bf16[768,512]{1,0:T(8,128)(2,1)S(1)} collective-permute-done((bf16[768,512]{1,0:T(8,128)(2,1)S(1)}, bf16[768,512]{1,0:T(8,128)(2,1)S(1)}, u32[]{:S(2)}, u32[]{:S(2)}) %collective-permute-start) | collective-permute-done | bytes 786464 | tf_op jit(solution)/shard_map/ppermute | solution.py:13
  55.3 8.5 %collective-permute-start.1 = (bf16[768,512]{1,0:T(8,128)(2,1)S(1)}, bf16[768,512]{1,0:T(8,128)(2,1)S(1)}, u32[]{:S(2)}, u32[]{:S(2)}) collective-permute-start(bf16[768,512]{1,0:T(8,128)(2,1)S(1)} %collective-permute-done), channel_id=1, source_target_pairs={{0,4},{4,8},{8,12},{12,0},{1,5},{5,9},{9,13},{13,1},{2,6},{6,10},{... | collective-permute-start | bytes 2359304 | tf_op jit(solution)/shard_map/ppermute | solution.py:13
  63.9 38.1 %collective-permute-done.1 = bf16[768,512]{1,0:T(8,128)(2,1)S(1)} collective-permute-done((bf16[768,512]{1,0:T(8,128)(2,1)S(1)}, bf16[768,512]{1,0:T(8,128)(2,1)S(1)}, u32[]{:S(2)}, u32[]{:S(2)}) %collective-permute-start.1) | collective-permute-done | bytes 786464 | tf_op jit(solution)/shard_map/ppermute | solution.py:13
  101.9 17.6 %collective-permute-start.2 = (bf16[768,512]{1,0:T(8,128)(2,1)S(1)}, bf16[768,512]{1,0:T(8,128)(2,1)S(1)}, u32[]{:S(2)}, u32[]{:S(2)}) collective-permute-start(bf16[768,512]{1,0:T(8,128)(2,1)S(1)} %collective-permute-done.1), channel_id=1, source_target_pairs={{0,4},{4,8},{8,12},{12,0},{1,5},{5,9},{9,13},{13,1},{2,6},{6,10},{... | collective-permute-start | bytes 2359304 | tf_op jit(solution)/shard_map/ppermute | solution.py:13
  119.6 36.6 %collective-permute-done.2 = bf16[768,512]{1,0:T(8,128)(2,1)S(1)} collective-permute-done((bf16[768,512]{1,0:T(8,128)(2,1)S(1)}, bf16[768,512]{1,0:T(8,128)(2,1)S(1)}, u32[]{:S(2)}, u32[]{:S(2)}) %collective-permute-start.2) | collective-permute-done | bytes 786464 | tf_op jit(solution)/shard_map/ppermute | solution.py:13
  156.1 1.0 constant_dynamic-update-slice_fusion.7
  157.1 1.0 constant_dynamic-update-slice_fusion.6
  158.1 1.0 constant_dynamic-update-slice_fusion.5
  159.1 0.9 constant_dynamic-update-slice_fusion.4
  160.0 1.0 constant_dynamic-update-slice_fusion.3
  161.0 18.9 %reduce-scatter.2.cloned.1.call-done = f32[512,768]{0,1:T(8,128)} async-done(((f32[2048,768]{0,1:T(8,128)}), f32[512,768]{0,1:T(8,128)}) %reduce-scatter.2.cloned.1.call-update) | async-done | bytes 1572880 | tf_op jit(solution)/shard_map/reduce_scatter | solution.py:34
  180.0 0.0 all-reduce.2.cloned.1.call-update
  180.0 0.0 copy-start.3
  180.0 0.0 copy-start.4
  180.0 1.0 constant_dynamic-update-slice_fusion.2
  181.0 1.0 constant_dynamic-update-slice_fusion.1
  182.0 1.0 constant_dynamic-update-slice_fusion
  183.0 0.0 copy-done.3
  183.0 0.0 copy-done.4
  183.0 7.7 %fusion.8 = (bf16[1024,768]{0,1:T(8,128)(2,1)S(1)}, bf16[1024,768]{0,1:T(8,128)(2,1)S(1)}) fusion(bf16[1024,768]{0,1:T(8,128)(2,1)S(1)} %copy-done.4, bf16[1024,768]{0,1:T(8,128)(2,1)S(1)} %copy-done.3, bf16[1024,2048]{1,0:T(8,128)(2,1)} %param.6, bf16[768,4096]{1,0:T(8,128)(2,1)} %constant_dynamic-update-slice_fusion, s32[]{:T(128)S(6)} %select_n.14), kind=kOutput, calls=%fused_computation.15 | convolution fusion | flops 3233021952 | bytes 13631492 | tf_op jit(solution)/shard_map/dot_general | solution.py:28
  190.7 1.6 copy.10
  192.2 1.6 copy.11
  193.8 39.4 %all-reduce.2.cloned.1.call-done = f32[512,768]{0,1:T(8,128)} async-done(((f32[512,768]{0,1:T(8,128)}), f32[512,768]{0,1:T(8,128)}) %all-reduce.2.cloned.1.call-update) | async-done | bytes 1572880 | tf_op jit(solution)/shard_map/psum | solution.py:42
  233.2 2.7 %multiply_reduce_fusion = (f32[768]{0:T(1024)S(1)}, f32[768,512]{1,0:T(8,128)}) fusion(f32[512,768]{0,1:T(8,128)} %all-reduce.2.cloned.1.call-done), kind=kLoop, calls=%fused_computation.18 | loop fusion | flops 1178880 | bytes 3148800 | tf_op jit(solution)/shard_map/reduce_sum | solution.py:44
  235.9 11.7 %psum.15 = f32[768]{0:T(1024)S(1)} all-reduce(f32[768]{0:T(1024)S(1)} %get-tuple-element.8), channel_id=1, replica_groups=mesh['rep'=2,'fs'=4,'tp'=4] {'fs'}, use_global_device_ids=true, to_apply=%region_3.4 | all-reduce | flops 768 | bytes 6144 | tf_op jit(solution)/shard_map/psum | solution.py:44
  247.6 0.6 broadcast_multiply_fusion
Async XLA Ops:
  7.2 1.9 copy-start.1
  7.2 172.8 %reduce-scatter.2.cloned.1.call-start = ((), (), s32[]{:S(2)}) async-start(), calls=%async_computation.1 | async-start | bytes 7864320 | tf_op jit(solution)/shard_map/reduce_scatter | solution.py:34
  9.1 10.6 %copy-start.2 = (bf16[1024,768]{0,1:T(8,128)(2,1)}, bf16[1024,768]{0,1:T(8,128)(2,1)S(1)}, u32[]{:S(2)}) copy-start(bf16[1024,768]{0,1:T(8,128)(2,1)S(1)} %copy.8) | copy-start | bytes 4718596
  19.7 1.1 copy-start
  19.7 213.5 %all-reduce.2.cloned.1.call-start = ((), (), s32[]{:S(2)}) async-start(), calls=%async_computation.2 | async-start | bytes 3145728 | tf_op jit(solution)/shard_map/psum | solution.py:42
  20.8 34.5 %collective-permute-start = (bf16[768,512]{1,0:T(8,128)(2,1)S(1)}, bf16[768,512]{1,0:T(8,128)(2,1)S(1)}, u32[]{:S(2)}, u32[]{:S(2)}) collective-permute-start(bf16[768,512]{1,0:T(8,128)(2,1)S(1)} %copy-done), channel_id=1, source_target_pairs={{0,4},{4,8},{8,12},{12,0},{1,5},{5,9},{9,13},{13,1},{2,6},{6,10},{... | collective-permute-start | bytes 2359304 | tf_op jit(solution)/shard_map/ppermute | solution.py:13
  55.3 46.6 %collective-permute-start.1 = (bf16[768,512]{1,0:T(8,128)(2,1)S(1)}, bf16[768,512]{1,0:T(8,128)(2,1)S(1)}, u32[]{:S(2)}, u32[]{:S(2)}) collective-permute-start(bf16[768,512]{1,0:T(8,128)(2,1)S(1)} %collective-permute-done), channel_id=1, source_target_pairs={{0,4},{4,8},{8,12},{12,0},{1,5},{5,9},{9,13},{13,1},{2,6},{6,10},{... | collective-permute-start | bytes 2359304 | tf_op jit(solution)/shard_map/ppermute | solution.py:13
  101.9 54.2 %collective-permute-start.2 = (bf16[768,512]{1,0:T(8,128)(2,1)S(1)}, bf16[768,512]{1,0:T(8,128)(2,1)S(1)}, u32[]{:S(2)}, u32[]{:S(2)}) collective-permute-start(bf16[768,512]{1,0:T(8,128)(2,1)S(1)} %collective-permute-done.1), channel_id=1, source_target_pairs={{0,4},{4,8},{8,12},{12,0},{1,5},{5,9},{9,13},{13,1},{2,6},{6,10},{... | collective-permute-start | bytes 2359304 | tf_op jit(solution)/shard_map/ppermute | solution.py:13
  180.0 3.0 %copy-start.3 = (bf16[1024,768]{0,1:T(8,128)(2,1)S(1)}, bf16[1024,768]{0,1:T(8,128)(2,1)}, u32[]{:S(2)}) copy-start(bf16[1024,768]{0,1:T(8,128)(2,1)} %copy-done.2) | copy-start | bytes 4718596
  180.0 3.0 %copy-start.4 = (bf16[1024,768]{0,1:T(8,128)(2,1)S(1)}, bf16[1024,768]{0,1:T(8,128)(2,1)}, u32[]{:S(2)}) copy-start(bf16[1024,768]{0,1:T(8,128)(2,1)} %copy.9) | copy-start | bytes 4718596
Sparse Core Ops, SparseCore 0:
  19.8 160.0 reduce-scatter.1
  182.3 50.9 all-reduce.1
